TPU v7x, 256 devices: a whole 4x4x8 slice. The times are simulated.
256 devices in a mesh: fs: 32 (over z, x), tp: 8 (over y, core).
Axes of the slice: x: 4, y: 4, z: 8, core: 2. Of those that a mesh axis runs over, the one named last changes fastest.
Arguments:
- tokens: bfloat16 [6144, 2048], P('fs'), may hold values from -6 to 6
- norm_gain: float32 [2048], P('fs'), may hold values from 0.1 to 1.9
- expert_gate: float32 [64, 2048, 1024], P(None, 'fs', 'tp'), may hold values from -0.125 to 0.125
- expert_up: float32 [64, 2048, 1024], P(None, 'fs', 'tp'), may hold values from -0.125 to 0.125
- expert_down: float32 [64, 1024, 2048], P(None, 'fs', 'tp'), may hold values from -0.1875 to 0.1875
- shared_gate: float32 [2048, 1024], P('fs', 'tp'), may hold values from -0.125 to 0.125
- shared_up: float32 [2048, 1024], P('fs', 'tp'), may hold values from -0.125 to 0.125
- shared_down: float32 [1024, 2048], P('fs', 'tp'), may hold values from -0.1875 to 0.1875
- expert_ids: int32 [6144, 8], P('fs'), may hold values from 0 to 63, all different within a row; in each aligned block of 192 rows (0 to 191, 192 to 383, ...) at most 48 rows name the same one
- route_weights: float32 [6144, 8], P('fs'), may hold values from 0.25 to 1
Outputs:
- gate_ready: bfloat16 [64, 2048, 1024], P('fs', None, 'tp')
- up_ready: bfloat16 [64, 2048, 1024], P('fs', None, 'tp')
- down_ready: bfloat16 [64, 1024, 2048], P('fs', None, 'tp')
- shared_gate_ready: bfloat16 [2048, 1024], P(None, 'tp')
- shared_up_ready: bfloat16 [2048, 1024], P(None, 'tp')
- shared_down_ready: bfloat16 [1024, 2048], P(None, 'tp')
- mixed: bfloat16 [6144, 2048], P('fs', 'tp')
Inputs may be any that keep to these rules, and one draw needn't show every extreme that they name: `expert_ids`: each row names 8 different experts. Among the 192 rows of one index of fs no expert is named more than 48 times, and in every draw some expert is named exactly 48 times there.
All inputs are finite; a program needn't handle non-finite values.
Results may differ from a plain program's by a relative error of at most 0.0085.
Values may be sent and summed in bfloat16 or wider, within the bound.
A program may use at most 128 MiB of HBM per device.

v0:
```python
import jax
import jax.numpy as jnp
from jax import lax
from jax.sharding import PartitionSpec as P

TOP_K = 8
EPS = 1e-06


def cut_along(shard, dim, size):
    before, after = (shard.shape[:dim], shard.shape[dim + 1 :])
    return jnp.moveaxis(shard.reshape(*before, size, -1, *after), dim, 0)


def piece_ends(length, count):
    turn = length // count
    if turn >= 8:
        turn -= turn % 8
    return [turn * k for k in range(1, count)]


def in_order(parts, dim):
    parts = jnp.moveaxis(parts, 0, dim)
    shape = parts.shape
    return parts.reshape(*shape[:dim], shape[dim] * shape[dim + 1], *shape[dim + 2 :])


def several_exchanges(shard, axis, pieces, split_dim, concat_dim):
    parts = cut_along(shard, split_dim, lax.axis_size(axis))
    split_at = max(range(1, max(2, parts.ndim - 1)), key=lambda d: parts.shape[d])
    done = []
    for share in jnp.split(parts, piece_ends(parts.shape[split_at], pieces), axis=split_at):
        if share.size:
            done.append(lax.all_to_all(share, axis, split_axis=0, concat_axis=0, tiled=True))
    return in_order(jnp.concatenate(done, axis=split_at), concat_dim)


def side_by_side(arrays, axis, dim, along):
    ends, at = ([], 0)
    for a in arrays[:-1]:
        at += a.shape[along]
        ends.append(at)
    both = jnp.concatenate(arrays, axis=along)
    return tuple(jnp.split(lax.all_gather(both, axis, axis=dim, tiled=True), ends, axis=along))


def turned_gather(arrays, axis, dims):
    turned = [jnp.moveaxis(a, dim, 0) for a, dim in zip(arrays, dims)]
    widths = [t[0].size for t in turned]
    both = jnp.concatenate([t.reshape(-1, w) for t, w in zip(turned, widths)], axis=1)
    result = lax.all_gather(both, axis, axis=0, tiled=True)
    parts = jnp.split(result, [sum(widths[:k]) for k in range(1, len(widths))], axis=1)
    return tuple(
        (
            jnp.moveaxis(b.reshape(-1, *t.shape[1:]), 0, dim)
            for b, t, dim in zip(parts, turned, dims)
        )
    )


def expert_hidden(rows, gate_new, up_new):
    first = jnp.einsum("secn,enf->secf", rows, gate_new, preferred_element_type=jnp.float32)
    second = jnp.einsum("secn,enf->secf", rows, up_new, preferred_element_type=jnp.float32)
    return (jax.nn.silu(first) * second).astype(jnp.bfloat16)


def body(
    tokens,
    norm_gain,
    expert_gate,
    expert_up,
    expert_down,
    shared_gate,
    shared_up,
    shared_down,
    expert_ids,
    route_weights,
):
    groups = lax.axis_size("fs")
    experts = expert_gate.shape[0]
    per_group = experts // groups
    tok_count = tokens.shape[0]
    capacity = 2 * tok_count * TOP_K // experts
    gate_local = (expert_gate * norm_gain[None, :, None]).astype(jnp.bfloat16)
    up_local = (expert_up * norm_gain[None, :, None]).astype(jnp.bfloat16)
    down_local = expert_down.astype(jnp.bfloat16)
    gate_local = gate_local.reshape((groups, per_group) + gate_local.shape[1:])
    up_local = up_local.reshape((groups, per_group) + up_local.shape[1:])
    down_local = down_local.reshape((groups, per_group) + down_local.shape[1:])
    shared_first_local = (shared_gate * norm_gain[:, None]).astype(jnp.bfloat16)
    shared_second_local = (shared_up * norm_gain[:, None]).astype(jnp.bfloat16)
    shared_third_local = shared_down.astype(jnp.bfloat16)
    gate_moved, up_moved = (
        several_exchanges(gate_local, "fs", 2, 0, 2),
        several_exchanges(up_local, "fs", 2, 0, 2),
    )
    gate_ready = gate_moved[0]
    up_ready = up_moved[0]
    shared_gate_ready, shared_up_ready, shared_down_ready = (
        *side_by_side((shared_first_local, shared_second_local), "fs", 0, 1),
        lax.all_gather(shared_third_local, "fs", axis=0, tiled=True),
    )
    wide = tokens.astype(jnp.float32)
    normed = (wide * lax.rsqrt(jnp.mean(wide * wide, axis=-1, keepdims=True) + EPS)).astype(
        jnp.bfloat16
    )
    chosen = expert_ids.reshape(-1)
    onehot = (chosen[:, None] == jnp.arange(experts, dtype=jnp.int32)[None, :]).astype(jnp.int32)
    ranks = jnp.sum(jnp.cumsum(onehot, axis=0) * onehot, axis=1) - 1
    owners = jnp.arange(tok_count * TOP_K, dtype=jnp.int32) // TOP_K
    slot_token = jnp.zeros((experts, capacity), jnp.int32).at[chosen, ranks].set(owners)
    outgoing = normed[slot_token.reshape(-1)].reshape(groups, per_group, capacity, normed.shape[1])
    share = capacity // lax.axis_size("tp")
    mine = lax.dynamic_slice_in_dim(outgoing, lax.axis_index("tp") * share, share, 2)
    arrived = lax.all_to_all(mine, "fs", split_axis=0, concat_axis=0, tiled=True)
    hidden = expert_hidden(lax.all_gather(arrived, "tp", axis=2, tiled=True), gate_ready, up_ready)
    shared_first = jnp.dot(normed, shared_gate_ready, preferred_element_type=jnp.float32)
    shared_second = jnp.dot(normed, shared_up_ready, preferred_element_type=jnp.float32)
    shared_hidden = (jax.nn.silu(shared_first) * shared_second).astype(jnp.bfloat16)[None, None]
    down_moved = lax.all_to_all(down_local, "fs", split_axis=0, concat_axis=2, tiled=True)
    down_ready = down_moved[0]
    columns = down_ready.shape[2]
    routed_piece, shared_piece = turned_gather((hidden, shared_hidden), "tp", (3, 3))
    routed_total = jnp.einsum(
        "secf,efd->secd", routed_piece, down_ready, preferred_element_type=jnp.float32
    )
    shared_total = jnp.einsum(
        "abtf,fd->abtd", shared_piece, shared_down_ready, preferred_element_type=jnp.float32
    )
    returned = lax.all_to_all(
        routed_total.astype(jnp.bfloat16), "fs", split_axis=0, concat_axis=0, tiled=True
    )
    returned = returned.reshape(experts * capacity, columns)
    picked = (
        returned[chosen * capacity + ranks].astype(jnp.float32).reshape(tok_count, TOP_K, columns)
    )
    routed = jnp.sum(picked * route_weights[:, :, None], axis=1)
    mixed = (shared_total[0, 0] + routed).astype(jnp.bfloat16)
    return (
        gate_ready,
        up_ready,
        down_ready,
        shared_gate_ready,
        shared_up_ready,
        shared_down_ready,
        mixed,
    )


def solution(mesh):
    in_specs = (
        P("fs", None),
        P("fs"),
        P(None, "fs", "tp"),
        P(None, "fs", "tp"),
        P(None, "fs", "tp"),
        P("fs", "tp"),
        P("fs", "tp"),
        P("fs", "tp"),
        P("fs", None),
        P("fs", None),
    )
    out_specs = (
        P("fs", None, "tp"),
        P("fs", None, "tp"),
        P("fs", None, "tp"),
        P(None, "tp"),
        P(None, "tp"),
        P(None, "tp"),
        P("fs", "tp"),
    )
    return jax.shard_map(body, mesh=mesh, in_specs=in_specs, out_specs=out_specs, check_vma=False)
```

profile of v0, /device:TPU:32, one launch (start us, length us, event | category | flops | bytes accessed | tf_op | source)
XLA Modules:
  0.0 414.8 jit_solution(16375426263147226016)
XLA Ops:
  7.2 0.8 copy.58
  8.0 0.1 eq.29
  8.1 0.1 eq.25
  8.2 0.1 reshape.182
  8.4 18.1 %reduce-window.6 = s32[64,12,128]{2,1,0:T(8,128)S(1)} reduce-window(s32[64,12,128]{2,1,0:T(8,128)S(1)} %fusion.25, s32[]{:T(128)} %constant.44.clone.1), window={size=1x1x128 pad=0_0x0_0x127_0}, to_apply=%region_1.0 | reduce-window | flops 12484608 | bytes 786436 | tf_op jit(solution)/shard_map/reduce-window
  26.5 0.2 slice.12
  26.7 0.3 copy.61
  27.0 0.1 copy.62
  27.1 0.2 broadcast_add_fusion
  27.3 0.1 fusion.27
  27.6 0.1 multiply_reduce_fusion
  27.7 0.1 and_reduce_fusion
  27.8 6.2 %scatter_custom_fusion = s32[3072]{0:T(1024)S(1)} fusion(s32[1536]{0:T(1024)S(1)} %get-tuple-element.23, s32[1536]{0:T(1024)S(1)} %get-tuple-element.22, s32[]{:T(128)} %constant.44.clone.1), kind=kCustom, calls=%fused_computation.63 | custom fusion | bytes 12292
  34.0 0.1 reshape.194
  34.0 0.1 copy.63
  34.1 0.1 reshape.184
  34.3 0.2 fusion.10
  34.5 0.2 fusion.11
  34.7 15.9 %gather_fusion = bf16[3072,2048]{1,0:T(8,128)(2,1)} fusion(bf16[192,2048]{1,0:T(8,128)(2,1)S(1)} %fusion.11, s32[3072]{0:T(1024)S(1)} %broadcast_clamp_fusion), kind=kCustom, calls=%fused_computation | custom fusion | bytes 25178112 | tf_op jit(solution)/shard_map/gather | solution.py:112
  50.7 3.0 constant_dynamic-slice_fusion
  53.7 2.8 copy.64
  56.5 11.3 %all-to-all-start.5 = ((bf16[32,2,6,2048]{3,1,2,0:T(2,128)(2,1)}), bf16[32,2,6,2048]{3,1,2,0:T(2,128)(2,1)S(1)}, u32[]{:S(2)}, u32[]{:S(2)}) async-start(bf16[32,2,6,2048]{3,1,2,0:T(2,128)(2,1)} %copy.64), calls=%async_computation.5 | async-start | bytes 3145728 | tf_op jit(solution)/shard_map/all_to_all | solution.py:115
  67.9 0.1 multiply_convert_fusion.3
  68.0 0.6 pad_maximum_fusion.1
  68.6 38.4 %all-to-all-done.5 = bf16[32,2,6,2048]{3,1,2,0:T(2,128)(2,1)S(1)} async-done(((bf16[32,2,6,2048]{3,1,2,0:T(2,128)(2,1)}), bf16[32,2,6,2048]{3,1,2,0:T(2,128)(2,1)S(1)}, u32[]{:S(2)}, u32[]{:S(2)}) %all-to-all-start.5) | async-done | bytes 1572896 | tf_op jit(solution)/shard_map/all_to_all | solution.py:115
  107.1 2.0 copy.65
  109.1 2.8 multiply_convert_fusion
  112.0 0.9 fusion.36
  112.9 23.9 %all_to_all.45 = bf16[32,1,2,32,128]{4,3,2,1,0:T(8,128)(2,1)S(1)} all-to-all(bf16[32,1,2,32,128]{4,3,2,1,0:T(8,128)(2,1)S(1)} %get-tuple-element.11), channel_id=1, replica_groups=mesh['fs'=32,'tp'=8] {'fs'}, dimensions={0} | all-to-all | bytes 1048576 | tf_op jit(solution)/shard_map/all_to_all | solution.py:34
  136.8 5.0 %all-to-all-start.1 = ((bf16[32,1,2,32,128]{4,3,2,1,0:T(8,128)(2,1)}), bf16[32,1,2,32,128]{4,3,2,1,0:T(8,128)(2,1)S(1)}, u32[]{:S(2)}, u32[]{:S(2)}) async-start(bf16[32,1,2,32,128]{4,3,2,1,0:T(8,128)(2,1)} %get-tuple-element.12), calls=%async_computation.1 | async-start | bytes 1048576 | tf_op jit(solution)/shard_map/all_to_all | solution.py:34
  141.8 0.9 fusion.35
  142.8 15.6 %all-to-all-done.1 = bf16[32,1,2,32,128]{4,3,2,1,0:T(8,128)(2,1)S(1)} async-done(((bf16[32,1,2,32,128]{4,3,2,1,0:T(8,128)(2,1)}), bf16[32,1,2,32,128]{4,3,2,1,0:T(8,128)(2,1)S(1)}, u32[]{:S(2)}, u32[]{:S(2)}) %all-to-all-start.1) | async-done | bytes 524320 | tf_op jit(solution)/shard_map/all_to_all | solution.py:34
  158.4 21.5 %all_to_all.46 = bf16[32,1,2,32,128]{4,3,2,1,0:T(8,128)(2,1)S(1)} all-to-all(bf16[32,1,2,32,128]{4,3,2,1,0:T(8,128)(2,1)S(1)} %get-tuple-element.9), channel_id=1, replica_groups=mesh['fs'=32,'tp'=8] {'fs'}, dimensions={0} | all-to-all | bytes 1048576 | tf_op jit(solution)/shard_map/all_to_all | solution.py:34
  179.9 5.1 %all-to-all-start.3 = ((bf16[32,1,2,32,128]{4,3,2,1,0:T(8,128)(2,1)}), bf16[32,1,2,32,128]{4,3,2,1,0:T(8,128)(2,1)S(1)}, u32[]{:S(2)}, u32[]{:S(2)}) async-start(bf16[32,1,2,32,128]{4,3,2,1,0:T(8,128)(2,1)} %get-tuple-element.10), calls=%async_computation.3 | async-start | bytes 1048576 | tf_op jit(solution)/shard_map/all_to_all | solution.py:34
  185.0 0.2 all-gather.8.cloned.1.call-start
  185.2 0.1 maximum_bitcast_fusion
  185.4 0.1 copy.55
  185.5 16.0 %all-to-all-done.3 = bf16[32,1,2,32,128]{4,3,2,1,0:T(8,128)(2,1)S(1)} async-done(((bf16[32,1,2,32,128]{4,3,2,1,0:T(8,128)(2,1)}), bf16[32,1,2,32,128]{4,3,2,1,0:T(8,128)(2,1)S(1)}, u32[]{:S(2)}, u32[]{:S(2)}) %all-to-all-start.3) | async-done | bytes 524320 | tf_op jit(solution)/shard_map/all_to_all | solution.py:34
  201.4 0.1 maximum_bitcast_fusion.1
  201.5 0.1 copy.56
  201.7 1.6 fusion.34
  203.3 0.4 fusion.37
  203.7 0.4 copy-done.6
  204.1 0.4 fusion.24
  204.5 18.0 %all-gather.6.cloned.1.call-done = bf16[32,2,48,2048]{3,0,1,2:T(8,128)(2,1)} async-done(((bf16[32,2,6,2048]{3,0,1,2:T(8,128)(2,1)}), bf16[32,2,48,2048]{3,0,1,2:T(8,128)(2,1)}) %all-gather.6.cloned.1.call-update) | async-done | bytes 12582928 | tf_op jit(solution)/shard_map/all_gather | solution.py:116
  222.5 18.0 %fusion.2 = f32[2,128,32,48]{1,3,2,0:T(8,128)S(1)} fusion(bf16[2,2048,128,1]{2,1,3,0:T(8,128)(2,1)S(1)} %bitcast.105, bf16[32,2,48,2048]{3,0,1,2:T(8,128)(2,1)} %all-gather.6.cloned.1.call-done), kind=kOutput, calls=%fused_computation.5 | convolution fusion | flops 1610612736 | bytes 15204352 | tf_op jit(solution)/shard_map/secn,enf->secf/dot_general | solution.py:62
  240.6 13.8 %fusion.13 = bf16[128,32,2,48]{0,3,1,2:T(8,128)(2,1)S(1)} fusion(f32[2,128,32,48]{1,3,2,0:T(8,128)S(1)} %fusion.2, bf16[2,2048,128,1]{2,1,3,0:T(8,128)(2,1)S(1)} %bitcast.107, bf16[32,2,48,2048]{3,0,1,2:T(8,128)(2,1)} %all-gather.6.cloned.1.call-done), kind=kOutput, calls=%fused_computation.20 | convolution fusion | flops 1612972032 | bytes 15990784 | tf_op jit(solution)/shard_map/secn,enf->secf/dot_general | solution.py:63
  254.3 0.1 copy.68
  254.4 0.9 pad_maximum_fusion
  255.4 0.9 copy-done.1
  256.2 0.1 convert_element_type.54
  256.4 37.4 %all_to_all.47 = bf16[32,2,32,256]{3,2,1,0:T(8,128)(2,1)S(1)} all-to-all(bf16[32,2,32,256]{3,2,1,0:T(8,128)(2,1)S(1)} %bitcast.101), channel_id=1, replica_groups=mesh['fs'=32,'tp'=8] {'fs'}, dimensions={0} | all-to-all | bytes 2097152 | tf_op jit(solution)/shard_map/all_to_all | solution.py:120
  293.8 0.1 copy.57
  293.9 10.6 %all-gather.8.cloned.1.call-done = bf16[1024,3264]{0,1:T(8,128)(2,1)} async-done(((bf16[128,3264]{0,1:T(8,128)(2,1)}), bf16[1024,3264]{0,1:T(8,128)(2,1)}) %all-gather.8.cloned.1.call-update) | async-done | bytes 6684688 | tf_op jit(solution)/shard_map/all_gather | solution.py:51
  304.6 2.8 slice-done
  307.4 1.8 fusion.17
  309.2 1.4 copy.70
  310.6 10.2 %all-to-all-start.6 = ((bf16[32,2,48,256]{3,2,1,0:T(8,128)(2,1)}), bf16[32,2,48,256]{3,2,1,0:T(8,128)(2,1)S(1)}, u32[]{:S(2)}, u32[]{:S(2)}) async-start(bf16[32,2,48,256]{3,2,1,0:T(8,128)(2,1)} %copy.70), calls=%async_computation.6 | async-start | bytes 3145728 | tf_op jit(solution)/shard_map/all_to_all | solution.py:130
  320.8 0.1 copy.71
  320.9 79.3 %all_gather.13 = bf16[1024,256]{1,0:T(8,128)(2,1)S(1)} all-gather(bf16[32,256]{1,0:T(8,128)(2,1)S(1)} %convert_element_type.57), channel_id=1, replica_groups=mesh['fs'=32,'tp'=8] {'fs'}, dimensions={0}, use_global_device_ids=true | all-gather | bytes 540672 | tf_op jit(solution)/shard_map/all_gather | solution.py:101
  400.3 4.8 %gather_fusion.1 = bf16[1536,256]{1,0:T(8,128)(2,1)S(1)} fusion(bf16[3072,256]{1,0:T(8,128)(2,1)S(1)} %bitcast.96, s32[2048]{0:T(1024)S(1)} %pad_clamp_fusion), kind=kCustom, calls=%fused_computation.1 | custom fusion | bytes 1579008 | tf_op jit(solution)/shard_map/gather | solution.py:135
  405.0 0.5 fusion.12
  405.6 1.9 fusion.22
  407.5 0.8 copy.92
  (44 shorter events, 0.4 us)
Async XLA Ops:
  8.3 19.2 %copy-start.13 = (s32[2]{0:T(128)S(1)}, s32[2]{0:T(128)}, u32[]{:S(2)}) copy-start(s32[2]{0:T(128)} %constant.57) | copy-start | bytes 28
  8.4 19.3 %copy-start.12 = (s32[2]{0:T(128)S(1)}, s32[2]{0:T(128)}, u32[]{:S(2)}) copy-start(s32[2]{0:T(128)} %constant.60) | copy-start | bytes 28
  8.4 25.9 %copy-start = (bf16[192,2048]{1,0:T(8,128)(2,1)S(1)}, bf16[192,2048]{1,0:T(8,128)(2,1)}, u32[]{:S(2)}) copy-start(bf16[192,2048]{1,0:T(8,128)(2,1)} %param.10) | copy-start | bytes 2359300
  56.5 11.4 %copy-start.7 = (f32[64,128]{1,0:T(8,128)S(1)}, f32[64,128]{1,0:T(8,128)}, u32[]{:S(2)}) copy-start(f32[64,128]{1,0:T(8,128)} %param.15) | copy-start | bytes 98308
  56.5 11.4 %copy-start.8 = (f32[64,128]{1,0:T(8,128)S(1)}, f32[64,128]{1,0:T(8,128)}, u32[]{:S(2)}) copy-start(f32[64,128]{1,0:T(8,128)} %param.16) | copy-start | bytes 98308
  56.5 11.4 %copy-start.11 = (f32[64]{0:T(128)S(1)}, f32[64]{0:T(128)}, u32[]{:S(2)}) copy-start(f32[64]{0:T(128)} %param.11) | copy-start | bytes 772
  56.5 50.6 %all-to-all-start.5 = ((bf16[32,2,6,2048]{3,1,2,0:T(2,128)(2,1)}), bf16[32,2,6,2048]{3,1,2,0:T(2,128)(2,1)S(1)}, u32[]{:S(2)}, u32[]{:S(2)}) async-start(bf16[32,2,6,2048]{3,1,2,0:T(2,128)(2,1)} %copy.64), calls=%async_computation.5 | async-start | bytes 3145728 | tf_op jit(solution)/shard_map/all_to_all | solution.py:115
  67.8 133.9 %all-gather.4.cloned.1.call-start = ((), (), s32[]{:S(2)}) async-start(), calls=%async_computation.7 | async-start | bytes 1081344 | tf_op jit(solution)/shard_map/all_gather | solution.py:44
  68.6 153.9 %all-gather.6.cloned.1.call-start = ((), (), s32[]{:S(2)}) async-start(), calls=%async_computation.8 | async-start | bytes 14155776 | tf_op jit(solution)/shard_map/all_gather | solution.py:116
  136.8 21.6 %all-to-all-start.1 = ((bf16[32,1,2,32,128]{4,3,2,1,0:T(8,128)(2,1)}), bf16[32,1,2,32,128]{4,3,2,1,0:T(8,128)(2,1)S(1)}, u32[]{:S(2)}, u32[]{:S(2)}) async-start(bf16[32,1,2,32,128]{4,3,2,1,0:T(8,128)(2,1)} %get-tuple-element.12), calls=%async_computation.1 | async-start | bytes 1048576 | tf_op jit(solution)/shard_map/all_to_all | solution.py:34
  179.9 21.5 %all-to-all-start.3 = ((bf16[32,1,2,32,128]{4,3,2,1,0:T(8,128)(2,1)}), bf16[32,1,2,32,128]{4,3,2,1,0:T(8,128)(2,1)S(1)}, u32[]{:S(2)}, u32[]{:S(2)}) async-start(bf16[32,1,2,32,128]{4,3,2,1,0:T(8,128)(2,1)} %get-tuple-element.10), calls=%async_computation.3 | async-start | bytes 1048576 | tf_op jit(solution)/shard_map/all_to_all | solution.py:34
  185.0 119.6 %all-gather.8.cloned.1.call-start = ((), (), s32[]{:S(2)}) async-start(), calls=%async_computation.9 | async-start | bytes 7520256 | tf_op jit(solution)/shard_map/all_gather | solution.py:51
  185.4 37.0 %copy-start.3 = (bf16[1,2,32,64,128]{4,3,2,1,0:T(8,128)(2,1)}, bf16[1,2,32,64,128]{4,3,2,1,0:T(8,128)(2,1)S(1)}, u32[]{:S(2)}) copy-start(bf16[1,2,32,64,128]{4,3,2,1,0:T(8,128)(2,1)S(1)} %copy.55) | copy-start | bytes 3145732
  201.6 38.9 %copy-start.4 = (bf16[1,2,32,64,128]{4,3,2,1,0:T(8,128)(2,1)}, bf16[1,2,32,64,128]{4,3,2,1,0:T(8,128)(2,1)S(1)}, u32[]{:S(2)}) copy-start(bf16[1,2,32,64,128]{4,3,2,1,0:T(8,128)(2,1)S(1)} %copy.56) | copy-start | bytes 3145732
  203.3 0.8 copy-start.6
  203.3 37.2 %copy-start.2 = (bf16[2048,128]{1,0:T(8,128)(2,1)}, bf16[2048,128]{1,0:T(8,128)(2,1)S(1)}, u32[]{:S(2)}) copy-start(bf16[2048,128]{1,0:T(8,128)(2,1)S(1)} %get-tuple-element.34) | copy-start | bytes 1572868
  254.3 1.9 copy-start.1
  293.9 10.7 %copy-start.5 = (bf16[1,2,32,32,256]{4,3,2,1,0:T(8,128)(2,1)}, bf16[1,2,32,32,256]{4,3,2,1,0:T(8,128)(2,1)S(1)}, u32[]{:S(2)}) copy-start(bf16[1,2,32,32,256]{4,3,2,1,0:T(8,128)(2,1)S(1)} %copy.57) | copy-start | bytes 3145732
  304.6 2.8 slice-start
  310.6 10.2 %copy-start.10 = (f32[192,8]{0,1:T(8,128)S(1)}, f32[192,8]{0,1:T(8,128)}, u32[]{:S(2)}) copy-start(f32[192,8]{0,1:T(8,128)} %param.19) | copy-start | bytes 18436
  310.6 10.3 %copy-start.9 = (f32[32,256]{1,0:T(8,128)S(1)}, f32[32,256]{1,0:T(8,128)}, u32[]{:S(2)}) copy-start(f32[32,256]{1,0:T(8,128)} %param.17) | copy-start | bytes 98308
  310.6 89.7 %all-to-all-start.6 = ((bf16[32,2,48,256]{3,2,1,0:T(8,128)(2,1)}), bf16[32,2,48,256]{3,2,1,0:T(8,128)(2,1)S(1)}, u32[]{:S(2)}, u32[]{:S(2)}) async-start(bf16[32,2,48,256]{3,2,1,0:T(8,128)(2,1)} %copy.70), calls=%async_computation.6 | async-start | bytes 3145728 | tf_op jit(solution)/shard_map/all_to_all | solution.py:130
Sparse Core Ops, SparseCore 0:
  71.8 80.5 all-gather.3
  154.2 68.2 all-gather.5
  255.5 49.0 all-gather.7
where the time goes:
time: 416 us; the launch traced here: 415 us
  blocking collectives  162 us (39%)
  waiting for transfers between devices  98.7 us (24%)
  local copies, waits for them, and re-layouts  46.8 us (11%)
  matrix products  36.3 us (9%)
  starting transfers between devices  31.9 us (8%)
  other arithmetic  24.6 us (6%)
  between operations  14.2 us (3%)
    all_gather x1, blocking collectives, body(): lax.all_gather(shared_third_local, 'fs', axis=0, tiled=True)  79.3 us
    all_to_all x2, blocking collectives, several_exchanges(): lax.all_to_all(share, axis, split_axis=0, concat_axis=0, tiled=True)  45.4 us
    all_to_all x1, waiting for transfers between devices, body(): lax.all_to_all(mine, 'fs', split_axis=0, concat_axis=0, tiled=True)  38.4 us
    all_to_all x1, blocking collectives, body(): lax.all_to_all(down_local, 'fs', split_axis=0, concat_axis=2, tiled=True)  37.4 us
    all_to_all x2, waiting for transfers between devices, several_exchanges(): lax.all_to_all(share, axis, split_axis=0, concat_axis=0, tiled=True)  31.6 us
    another operation x3, other arithmetic  18.4 us
    dot_general x1, matrix products, expert_hidden(): jnp.einsum('secn,enf->secf', rows, gate_new, preferred_element_type=jnp.f...  18 us
    all_gather x1, waiting for transfers between devices, body(): lax.all_gather(arrived, 'tp', axis=2, tiled=True)  18 us
  transfers between devices with their start and end apart: 7, of which 5 were waited for; matrix products, arithmetic and copies ran while one was open for 3% of the time, Pallas kernels for 0%

commit v1 on v0

--- a/solution.py
+++ b/solution.py
@@ -5,6 +5,15 @@
 
 TOP_K = 8
 EPS = 1e-06
+
+
+def reach_copies_over_axis(x0, in_dim=0):
+    return jnp.concatenate(
+        jax.lax.all_to_all(
+            jnp.stack([x0 for _ in range(jax.lax.axis_size("fs"))], axis=0), "fs", 0, 0
+        ),
+        axis=in_dim,
+    )
 
 
 def cut_along(shard, dim, size):
@@ -98,7 +107,7 @@
     up_ready = up_moved[0]
     shared_gate_ready, shared_up_ready, shared_down_ready = (
         *side_by_side((shared_first_local, shared_second_local), "fs", 0, 1),
-        lax.all_gather(shared_third_local, "fs", axis=0, tiled=True),
+        reach_copies_over_axis(shared_third_local),
     )
     wide = tokens.astype(jnp.float32)
     normed = (wide * lax.rsqrt(jnp.mean(wide * wide, axis=-1, keepdims=True) + EPS)).astype(

time: 416 us -> 378 us (0.909)
  blocking collectives: 162 us -> 45.4 us
  waiting for transfers between devices: 98.7 us -> 163 us
  starting transfers between devices: 31.9 us -> 43.4 us
    all_gather x1 -> x0, blocking collectives: 79.3 us -> none  [body(): lax.all_gather(shared_third_local, 'fs', axis=0, tiled=True)]
    all_to_all x1 -> x0, blocking collectives: 37.4 us -> none  [body(): lax.all_to_all(down_local, 'fs', split_axis=0, concat_axis=2, tiled=True)]
    all_to_all x1, waiting for transfers between devices: 0.01 us -> 37.3 us  [body(): lax.all_to_all(routed_total.astype(jnp.bfloat16), 'fs', split_axis=0, con...]
    all_to_all x0 -> x2, waiting for transfers between devices: none -> 35.6 us  [the longest x1 27.6 us: body(): lax.all_to_all(down_local, 'fs', split_axis=0, concat_axis=2, tiled=True)]
    all_to_all x0 -> x2, starting transfers between devices: none -> 16.5 us  [the longest x1 10.1 us: body(): lax.all_to_all(down_local, 'fs', split_axis=0, concat_axis=2, tiled=True)]
    all_gather x1, waiting for transfers between devices: 10.6 us -> 2.14 us  [turned_gather(): result = lax.all_gather(both, axis, axis=0, tiled=True)]
    all_to_all x1, starting transfers between devices: 10.2 us -> 5.12 us  [body(): lax.all_to_all(routed_total.astype(jnp.bfloat16), 'fs', split_axis=0, con...]
  transfers between devices with their start and end apart: 7 -> 9, of which waited for: 5 -> 8; matrix products, arithmetic and copies ran while one was open for 3% -> 4% of each run, Pallas kernels for 0% -> 0%
where the time goes in v1:
time: 378 us; the launch traced here: 376 us
  waiting for transfers between devices  163 us (43%)
  local copies, waits for them, and re-layouts  47.7 us (13%)
  blocking collectives  45.4 us (12%)
  starting transfers between devices  43.4 us (11%)
  matrix products  36.3 us (10%)
  other arithmetic  25.6 us (7%)
  between operations  14.2 us (4%)
    all_to_all x2, blocking collectives, several_exchanges(): lax.all_to_all(share, axis, split_axis=0, concat_axis=0, tiled=True)  45.4 us
    all_to_all x1, waiting for transfers between devices, body(): lax.all_to_all(mine, 'fs', split_axis=0, concat_axis=0, tiled=True)  38.4 us
    all_to_all x1, waiting for transfers between devices, body(): lax.all_to_all(routed_total.astype(jnp.bfloat16), 'fs', split_axis=0, con...  37.3 us
    all_to_all x2, waiting for transfers between devices, several_exchanges(): lax.all_to_all(share, axis, split_axis=0, concat_axis=0, tiled=True)  31.6 us
    all_to_all x1, waiting for transfers between devices, body(): lax.all_to_all(down_local, 'fs', split_axis=0, concat_axis=2, tiled=True)  27.6 us
    another operation x3, other arithmetic  18.4 us
    dot_general x1, matrix products, expert_hidden(): jnp.einsum('secn,enf->secf', rows, gate_new, preferred_element_type=jnp.f...  18 us
    all_gather x1, waiting for transfers between devices, body(): lax.all_gather(arrived, 'tp', axis=2, tiled=True)  18 us
  transfers between devices with their start and end apart: 9, of which 8 were waited for; matrix products, arithmetic and copies ran while one was open for 4% of the time, Pallas kernels for 0%

profile of v1, /device:TPU:32, one launch (start us, length us, event | category | flops | bytes accessed | tf_op | source)
XLA Modules:
  0.0 375.7 jit_solution(5297712242450986957)
XLA Ops:
  7.2 0.8 copy.58
  8.0 0.1 eq.29
  8.1 0.1 eq.25
  8.2 0.1 reshape.188
  8.4 18.1 %reduce-window.6 = s32[64,12,128]{2,1,0:T(8,128)S(1)} reduce-window(s32[64,12,128]{2,1,0:T(8,128)S(1)} %fusion.25, s32[]{:T(128)} %constant.44.clone.1), window={size=1x1x128 pad=0_0x0_0x127_0}, to_apply=%region_1.0 | reduce-window | flops 12484608 | bytes 786436 | tf_op jit(solution)/shard_map/reduce-window
  26.5 0.2 slice.12
  26.7 0.3 copy.61
  27.0 0.1 copy.62
  27.1 0.2 broadcast_add_fusion
  27.3 0.1 fusion.27
  27.6 0.1 multiply_reduce_fusion
  27.7 0.1 and_reduce_fusion
  27.8 6.2 %scatter_custom_fusion = s32[3072]{0:T(1024)S(1)} fusion(s32[1536]{0:T(1024)S(1)} %get-tuple-element.23, s32[1536]{0:T(1024)S(1)} %get-tuple-element.22, s32[]{:T(128)} %constant.44.clone.1), kind=kCustom, calls=%fused_computation.63 | custom fusion | bytes 12292
  34.0 0.1 copy.63
  34.1 0.1 reshape.190
  34.3 0.2 fusion.10
  34.5 0.2 fusion.11
  34.7 15.9 %gather_fusion = bf16[3072,2048]{1,0:T(8,128)(2,1)} fusion(bf16[192,2048]{1,0:T(8,128)(2,1)S(1)} %fusion.11, s32[3072]{0:T(1024)S(1)} %broadcast_clamp_fusion), kind=kCustom, calls=%fused_computation | custom fusion | bytes 25178112 | tf_op jit(solution)/shard_map/gather | solution.py:121
  50.6 3.0 constant_dynamic-slice_fusion
  53.6 2.8 copy.64
  56.4 11.3 %all-to-all-start.6 = ((bf16[32,2,6,2048]{3,1,2,0:T(2,128)(2,1)}), bf16[32,2,6,2048]{3,1,2,0:T(2,128)(2,1)S(1)}, u32[]{:S(2)}, u32[]{:S(2)}) async-start(bf16[32,2,6,2048]{3,1,2,0:T(2,128)(2,1)} %copy.64), calls=%async_computation.6 | async-start | bytes 3145728 | tf_op jit(solution)/shard_map/all_to_all | solution.py:124
  67.9 0.6 pad_maximum_fusion.1
  68.6 38.4 %all-to-all-done.6 = bf16[32,2,6,2048]{3,1,2,0:T(2,128)(2,1)S(1)} async-done(((bf16[32,2,6,2048]{3,1,2,0:T(2,128)(2,1)}), bf16[32,2,6,2048]{3,1,2,0:T(2,128)(2,1)S(1)}, u32[]{:S(2)}, u32[]{:S(2)}) %all-to-all-start.6) | async-done | bytes 1572896 | tf_op jit(solution)/shard_map/all_to_all | solution.py:124
  107.1 2.1 copy.65
  109.1 2.8 multiply_convert_fusion
  112.0 0.9 fusion.36
  112.9 23.9 %all_to_all.50 = bf16[32,1,2,32,128]{4,3,2,1,0:T(8,128)(2,1)S(1)} all-to-all(bf16[32,1,2,32,128]{4,3,2,1,0:T(8,128)(2,1)S(1)} %get-tuple-element.11), channel_id=1, replica_groups=mesh['fs'=32,'tp'=8] {'fs'}, dimensions={0} | all-to-all | bytes 1048576 | tf_op jit(solution)/shard_map/all_to_all | solution.py:43
  136.8 5.0 %all-to-all-start.1 = ((bf16[32,1,2,32,128]{4,3,2,1,0:T(8,128)(2,1)}), bf16[32,1,2,32,128]{4,3,2,1,0:T(8,128)(2,1)S(1)}, u32[]{:S(2)}, u32[]{:S(2)}) async-start(bf16[32,1,2,32,128]{4,3,2,1,0:T(8,128)(2,1)} %get-tuple-element.12), calls=%async_computation.1 | async-start | bytes 1048576 | tf_op jit(solution)/shard_map/all_to_all | solution.py:43
  141.8 0.9 fusion.35
  142.8 15.6 %all-to-all-done.1 = bf16[32,1,2,32,128]{4,3,2,1,0:T(8,128)(2,1)S(1)} async-done(((bf16[32,1,2,32,128]{4,3,2,1,0:T(8,128)(2,1)}), bf16[32,1,2,32,128]{4,3,2,1,0:T(8,128)(2,1)S(1)}, u32[]{:S(2)}, u32[]{:S(2)}) %all-to-all-start.1) | async-done | bytes 524320 | tf_op jit(solution)/shard_map/all_to_all | solution.py:43
  158.4 21.5 %all_to_all.51 = bf16[32,1,2,32,128]{4,3,2,1,0:T(8,128)(2,1)S(1)} all-to-all(bf16[32,1,2,32,128]{4,3,2,1,0:T(8,128)(2,1)S(1)} %get-tuple-element.9), channel_id=1, replica_groups=mesh['fs'=32,'tp'=8] {'fs'}, dimensions={0} | all-to-all | bytes 1048576 | tf_op jit(solution)/shard_map/all_to_all | solution.py:43
  179.9 5.1 %all-to-all-start.3 = ((bf16[32,1,2,32,128]{4,3,2,1,0:T(8,128)(2,1)}), bf16[32,1,2,32,128]{4,3,2,1,0:T(8,128)(2,1)S(1)}, u32[]{:S(2)}, u32[]{:S(2)}) async-start(bf16[32,1,2,32,128]{4,3,2,1,0:T(8,128)(2,1)} %get-tuple-element.10), calls=%async_computation.3 | async-start | bytes 1048576 | tf_op jit(solution)/shard_map/all_to_all | solution.py:43
  185.0 0.2 all-gather.8.cloned.1.call-start
  185.2 0.1 maximum_bitcast_fusion
  185.4 0.1 copy.55
  185.5 16.0 %all-to-all-done.3 = bf16[32,1,2,32,128]{4,3,2,1,0:T(8,128)(2,1)S(1)} async-done(((bf16[32,1,2,32,128]{4,3,2,1,0:T(8,128)(2,1)}), bf16[32,1,2,32,128]{4,3,2,1,0:T(8,128)(2,1)S(1)}, u32[]{:S(2)}, u32[]{:S(2)}) %all-to-all-start.3) | async-done | bytes 524320 | tf_op jit(solution)/shard_map/all_to_all | solution.py:43
  201.4 0.1 maximum_bitcast_fusion.1
  201.5 0.1 copy.56
  201.7 1.6 fusion.34
  203.3 0.4 fusion.37
  203.7 0.4 copy-done.6
  204.1 0.4 fusion.24
  204.5 18.0 %all-gather.6.cloned.1.call-done = bf16[32,2,48,2048]{3,0,1,2:T(8,128)(2,1)} async-done(((bf16[32,2,6,2048]{3,0,1,2:T(8,128)(2,1)}), bf16[32,2,48,2048]{3,0,1,2:T(8,128)(2,1)}) %all-gather.6.cloned.1.call-update) | async-done | bytes 12582928 | tf_op jit(solution)/shard_map/all_gather | solution.py:125
  222.5 18.0 %fusion.2 = f32[2,128,32,48]{1,3,2,0:T(8,128)S(1)} fusion(bf16[2,2048,128,1]{2,1,3,0:T(8,128)(2,1)S(1)} %bitcast.107, bf16[32,2,48,2048]{3,0,1,2:T(8,128)(2,1)} %all-gather.6.cloned.1.call-done), kind=kOutput, calls=%fused_computation.5 | convolution fusion | flops 1610612736 | bytes 15204352 | tf_op jit(solution)/shard_map/secn,enf->secf/dot_general | solution.py:71
  240.6 13.8 %fusion.13 = bf16[128,32,2,48]{0,3,1,2:T(8,128)(2,1)S(1)} fusion(f32[2,128,32,48]{1,3,2,0:T(8,128)S(1)} %fusion.2, bf16[2,2048,128,1]{2,1,3,0:T(8,128)(2,1)S(1)} %bitcast.109, bf16[32,2,48,2048]{3,0,1,2:T(8,128)(2,1)} %all-gather.6.cloned.1.call-done), kind=kOutput, calls=%fused_computation.20 | convolution fusion | flops 1612972032 | bytes 15990784 | tf_op jit(solution)/shard_map/secn,enf->secf/dot_general | solution.py:72
  254.4 0.9 pad_maximum_fusion
  255.4 0.9 copy-done.1
  256.2 1.1 convert_element_type.54
  257.4 10.1 %all-to-all-start.4 = ((bf16[32,2,32,256]{3,2,1,0:T(8,128)(2,1)}), bf16[32,2,32,256]{3,2,1,0:T(8,128)(2,1)S(1)}, u32[]{:S(2)}, u32[]{:S(2)}) async-start(bf16[32,2,32,256]{3,2,1,0:T(8,128)(2,1)} %bitcast.6), calls=%async_computation.4 | async-start | bytes 2097152 | tf_op jit(solution)/shard_map/all_to_all | solution.py:129
  267.4 27.6 %all-to-all-done.4 = bf16[32,2,32,256]{3,2,1,0:T(8,128)(2,1)S(1)} async-done(((bf16[32,2,32,256]{3,2,1,0:T(8,128)(2,1)}), bf16[32,2,32,256]{3,2,1,0:T(8,128)(2,1)S(1)}, u32[]{:S(2)}, u32[]{:S(2)}) %all-to-all-start.4) | async-done | bytes 1048608 | tf_op jit(solution)/shard_map/all_to_all | solution.py:129
  295.0 0.9 stack.2
  295.9 6.5 %all-to-all-start.5 = ((bf16[32,32,256]{2,1,0:T(8,128)(2,1)}), bf16[32,32,256]{2,1,0:T(8,128)(2,1)S(1)}, u32[]{:S(2)}, u32[]{:S(2)}) async-start(bf16[32,32,256]{2,1,0:T(8,128)(2,1)} %stack.2), calls=%async_computation.5 | async-start | bytes 1048576 | tf_op jit(solution)/shard_map/all_to_all | solution.py:12
  302.4 2.1 all-gather.8.cloned.1.call-done
  304.6 2.8 slice-done
  307.4 1.8 fusion.17
  309.2 1.4 copy.70
  310.6 8.0 %all-to-all-done.5 = bf16[32,32,256]{2,1,0:T(8,128)(2,1)S(1)} async-done(((bf16[32,32,256]{2,1,0:T(8,128)(2,1)}), bf16[32,32,256]{2,1,0:T(8,128)(2,1)S(1)}, u32[]{:S(2)}, u32[]{:S(2)}) %all-to-all-start.5) | async-done | bytes 524320 | tf_op jit(solution)/shard_map/all_to_all | solution.py:12
  318.6 5.1 %all-to-all-start.7 = ((bf16[32,2,48,256]{3,2,1,0:T(8,128)(2,1)}), bf16[32,2,48,256]{3,2,1,0:T(8,128)(2,1)S(1)}, u32[]{:S(2)}, u32[]{:S(2)}) async-start(bf16[32,2,48,256]{3,2,1,0:T(8,128)(2,1)} %copy.70), calls=%async_computation.7 | async-start | bytes 3145728 | tf_op jit(solution)/shard_map/all_to_all | solution.py:139
  323.8 0.1 copy.71
  323.9 37.3 %all-to-all-done.7 = bf16[32,2,48,256]{3,2,1,0:T(8,128)(2,1)S(1)} async-done(((bf16[32,2,48,256]{3,2,1,0:T(8,128)(2,1)}), bf16[32,2,48,256]{3,2,1,0:T(8,128)(2,1)S(1)}, u32[]{:S(2)}, u32[]{:S(2)}) %all-to-all-start.7) | async-done | bytes 1572896 | tf_op jit(solution)/shard_map/all_to_all | solution.py:139
  361.2 4.8 %gather_fusion.1 = bf16[1536,256]{1,0:T(8,128)(2,1)S(1)} fusion(bf16[3072,256]{1,0:T(8,128)(2,1)S(1)} %bitcast.97, s32[2048]{0:T(1024)S(1)} %pad_clamp_fusion), kind=kCustom, calls=%fused_computation.1 | custom fusion | bytes 1579008 | tf_op jit(solution)/shard_map/gather | solution.py:144
  366.0 0.5 fusion.12
  366.5 1.9 fusion.22
  368.4 0.8 copy.92
  (47 shorter events, 0.7 us)
Async XLA Ops:
  8.3 19.2 %copy-start.13 = (s32[2]{0:T(128)S(1)}, s32[2]{0:T(128)}, u32[]{:S(2)}) copy-start(s32[2]{0:T(128)} %constant.57) | copy-start | bytes 28
  8.4 19.3 %copy-start.12 = (s32[2]{0:T(128)S(1)}, s32[2]{0:T(128)}, u32[]{:S(2)}) copy-start(s32[2]{0:T(128)} %constant.60) | copy-start | bytes 28
  8.4 25.9 %copy-start = (bf16[192,2048]{1,0:T(8,128)(2,1)S(1)}, bf16[192,2048]{1,0:T(8,128)(2,1)}, u32[]{:S(2)}) copy-start(bf16[192,2048]{1,0:T(8,128)(2,1)} %param.10) | copy-start | bytes 2359300
  56.4 11.4 %copy-start.7 = (f32[64,128]{1,0:T(8,128)S(1)}, f32[64,128]{1,0:T(8,128)}, u32[]{:S(2)}) copy-start(f32[64,128]{1,0:T(8,128)} %param.15) | copy-start | bytes 98308
  56.4 11.4 %copy-start.8 = (f32[64,128]{1,0:T(8,128)S(1)}, f32[64,128]{1,0:T(8,128)}, u32[]{:S(2)}) copy-start(f32[64,128]{1,0:T(8,128)} %param.16) | copy-start | bytes 98308
  56.4 11.4 %copy-start.11 = (f32[64]{0:T(128)S(1)}, f32[64]{0:T(128)}, u32[]{:S(2)}) copy-start(f32[64]{0:T(128)} %param.11) | copy-start | bytes 772
  56.4 50.6 %all-to-all-start.6 = ((bf16[32,2,6,2048]{3,1,2,0:T(2,128)(2,1)}), bf16[32,2,6,2048]{3,1,2,0:T(2,128)(2,1)S(1)}, u32[]{:S(2)}, u32[]{:S(2)}) async-start(bf16[32,2,6,2048]{3,1,2,0:T(2,128)(2,1)} %copy.64), calls=%async_computation.6 | async-start | bytes 3145728 | tf_op jit(solution)/shard_map/all_to_all | solution.py:124
  67.8 133.9 %all-gather.4.cloned.1.call-start = ((), (), s32[]{:S(2)}) async-start(), calls=%async_computation.8 | async-start | bytes 1081344 | tf_op jit(solution)/shard_map/all_gather | solution.py:53
  68.6 153.9 %all-gather.6.cloned.1.call-start = ((), (), s32[]{:S(2)}) async-start(), calls=%async_computation.9 | async-start | bytes 14155776 | tf_op jit(solution)/shard_map/all_gather | solution.py:125
  136.8 21.6 %all-to-all-start.1 = ((bf16[32,1,2,32,128]{4,3,2,1,0:T(8,128)(2,1)}), bf16[32,1,2,32,128]{4,3,2,1,0:T(8,128)(2,1)S(1)}, u32[]{:S(2)}, u32[]{:S(2)}) async-start(bf16[32,1,2,32,128]{4,3,2,1,0:T(8,128)(2,1)} %get-tuple-element.12), calls=%async_computation.1 | async-start | bytes 1048576 | tf_op jit(solution)/shard_map/all_to_all | solution.py:43
  179.9 21.5 %all-to-all-start.3 = ((bf16[32,1,2,32,128]{4,3,2,1,0:T(8,128)(2,1)}), bf16[32,1,2,32,128]{4,3,2,1,0:T(8,128)(2,1)S(1)}, u32[]{:S(2)}, u32[]{:S(2)}) async-start(bf16[32,1,2,32,128]{4,3,2,1,0:T(8,128)(2,1)} %get-tuple-element.10), calls=%async_computation.3 | async-start | bytes 1048576 | tf_op jit(solution)/shard_map/all_to_all | solution.py:43
  185.0 119.6 %all-gather.8.cloned.1.call-start = ((), (), s32[]{:S(2)}) async-start(), calls=%async_computation.10 | async-start | bytes 7520256 | tf_op jit(solution)/shard_map/all_gather | solution.py:60
  185.4 37.0 %copy-start.3 = (bf16[1,2,32,64,128]{4,3,2,1,0:T(8,128)(2,1)}, bf16[1,2,32,64,128]{4,3,2,1,0:T(8,128)(2,1)S(1)}, u32[]{:S(2)}) copy-start(bf16[1,2,32,64,128]{4,3,2,1,0:T(8,128)(2,1)S(1)} %copy.55) | copy-start | bytes 3145732
  201.6 38.9 %copy-start.4 = (bf16[1,2,32,64,128]{4,3,2,1,0:T(8,128)(2,1)}, bf16[1,2,32,64,128]{4,3,2,1,0:T(8,128)(2,1)S(1)}, u32[]{:S(2)}) copy-start(bf16[1,2,32,64,128]{4,3,2,1,0:T(8,128)(2,1)S(1)} %copy.56) | copy-start | bytes 3145732
  203.3 0.8 copy-start.6
  203.3 37.2 %copy-start.2 = (bf16[2048,128]{1,0:T(8,128)(2,1)}, bf16[2048,128]{1,0:T(8,128)(2,1)S(1)}, u32[]{:S(2)}) copy-start(bf16[2048,128]{1,0:T(8,128)(2,1)S(1)} %get-tuple-element.34) | copy-start | bytes 1572868
  254.3 1.9 copy-start.1
  256.2 11.2 %copy-start.9 = (f32[32,256]{1,0:T(8,128)S(1)}, f32[32,256]{1,0:T(8,128)}, u32[]{:S(2)}) copy-start(f32[32,256]{1,0:T(8,128)} %param.17) | copy-start | bytes 98308
  257.4 37.7 %all-to-all-start.4 = ((bf16[32,2,32,256]{3,2,1,0:T(8,128)(2,1)}), bf16[32,2,32,256]{3,2,1,0:T(8,128)(2,1)S(1)}, u32[]{:S(2)}, u32[]{:S(2)}) async-start(bf16[32,2,32,256]{3,2,1,0:T(8,128)(2,1)} %bitcast.6), calls=%async_computation.4 | async-start | bytes 2097152 | tf_op jit(solution)/shard_map/all_to_all | solution.py:129
  295.9 22.8 %all-to-all-start.5 = ((bf16[32,32,256]{2,1,0:T(8,128)(2,1)}), bf16[32,32,256]{2,1,0:T(8,128)(2,1)S(1)}, u32[]{:S(2)}, u32[]{:S(2)}) async-start(bf16[32,32,256]{2,1,0:T(8,128)(2,1)} %stack.2), calls=%async_computation.5 | async-start | bytes 1048576 | tf_op jit(solution)/shard_map/all_to_all | solution.py:12
  302.4 2.2 copy-start.5
  304.6 2.8 slice-start
  310.6 13.2 %copy-start.10 = (f32[192,8]{0,1:T(8,128)S(1)}, f32[192,8]{0,1:T(8,128)}, u32[]{:S(2)}) copy-start(f32[192,8]{0,1:T(8,128)} %param.19) | copy-start | bytes 18436
  318.6 42.6 %all-to-all-start.7 = ((bf16[32,2,48,256]{3,2,1,0:T(8,128)(2,1)}), bf16[32,2,48,256]{3,2,1,0:T(8,128)(2,1)S(1)}, u32[]{:S(2)}, u32[]{:S(2)}) async-start(bf16[32,2,48,256]{3,2,1,0:T(8,128)(2,1)} %copy.70), calls=%async_computation.7 | async-start | bytes 3145728 | tf_op jit(solution)/shard_map/all_to_all | solution.py:139
Sparse Core Ops, SparseCore 0:
  71.7 80.5 all-gather.3
  154.2 68.2 all-gather.5
  255.5 49.0 all-gather.7
